TPU v7x, 32 devices: a whole 2x2x4 slice. The times are simulated.
32 devices in a mesh: gr: 2 (over x), sp: 8 (over z, y), tp: 2 (over core).
Axes of the slice: x: 2, y: 2, z: 4, core: 2. Of those that a mesh axis runs over, the one named last changes fastest.
Arguments:
- tokens: bfloat16 [2, 2, 6144, 2048], P('gr', 'tp', 'sp'), may hold values from -6 to 6
- key_weight: bfloat16 [2048, 2048], replicated, may hold values from -0.125 to 0.125
- value_weight: bfloat16 [2048, 2048], replicated, may hold values from -0.125 to 0.125
- cum_gate: float32 [2, 32, 2, 6144], P('gr', None, 'tp', 'sp'), may hold values from -12588 to 0, as said below
- query: bfloat16 [2, 32, 64], P('gr', 'sp'), may hold values from -12 to 12
Outputs:
- kv_cache: bfloat16 [2, 32, 12288, 128], P('gr', 'sp', 'tp')
- gate_cache: float32 [2, 32, 12288], P('gr', 'sp', 'tp')
- read: bfloat16 [2, 32, 64], P('gr', 'sp')
Inputs may be any that keep to these rules, and one draw needn't show every extreme that they name: `cum_gate`: each head's entries never rise along the positions.
All inputs are finite; a program needn't handle non-finite values.
Results may differ from a plain program's by a relative error of at most 0.012.
Values may be sent and summed in bfloat16 or wider, within the bound.
A program may use at most 128 MiB of HBM per device.

v0:
```python
import jax
import jax.numpy as jnp
from jax import lax
from jax.sharding import PartitionSpec as P


def merged(value, axis, join):
    pieces = jax.tree.map(lambda part: lax.all_gather(part, axis), value)
    head = jax.tree.map(lambda part: part[0], pieces)
    tail = jax.tree.map(lambda part: part[1:], pieces)
    subtotal, _ = lax.scan(lambda subtotal, share: (join(subtotal, share), None), head, tail)
    return subtotal


def combine_reads(first, second):
    top = jnp.maximum(first[0], second[0])
    scale_one = jnp.exp(first[0] - top)
    scale_two = jnp.exp(second[0] - top)
    total = first[1] * scale_one + second[1] * scale_two
    weighted = first[2] * scale_one[..., None] + second[2] * scale_two[..., None]
    return (top, total, weighted)


def partial_read(query, keys, values, gates, head_size):
    scores = jnp.einsum("bhe,bhse->bhs", query, keys, preferred_element_type=jnp.float32)
    scores = scores * head_size ** (-0.5) - gates
    top = jnp.max(scores, axis=-1)
    weights = jnp.exp(scores - top[..., None])
    total = jnp.sum(weights, axis=-1)
    weighted = jnp.einsum(
        "bhs,bhse->bhe", weights.astype(jnp.bfloat16), values, preferred_element_type=jnp.float32
    )
    return (top, total, weighted)


def local_project(tokens, key_weight, value_weight, head_size):
    width = tokens.shape[3]
    local_rows = tokens[:, 0]
    key_part = jnp.einsum(
        "btd,dhe->bhte",
        local_rows,
        key_weight.reshape(width, -1, head_size),
        preferred_element_type=jnp.float32,
    ).astype(jnp.bfloat16)
    value_part = jnp.einsum(
        "btd,dhe->bhte",
        local_rows,
        value_weight.reshape(width, -1, head_size),
        preferred_element_type=jnp.float32,
    ).astype(jnp.bfloat16)
    return (key_part, value_part)


def on_device(tokens, key_weight, value_weight, cum_gate, query):
    count = tokens.shape[0]
    head_size = query.shape[2]
    key_part = None
    value_part = None
    key_part, value_part = local_project(tokens, key_weight, value_weight, head_size)
    joined = jnp.concatenate([key_part, value_part], axis=-1)
    kv_cache = lax.all_to_all(joined, "sp", split_axis=1, concat_axis=2, tiled=True)
    gates = lax.all_to_all(cum_gate, "sp", split_axis=1, concat_axis=3, tiled=True)
    gate_cache = gates.reshape(count, gates.shape[1], gates.shape[3])
    parts = partial_read(
        query, kv_cache[..., :head_size], kv_cache[..., head_size:], gate_cache, head_size
    )
    top, total, weighted = merged(parts, "tp", combine_reads)
    read = (weighted / total[..., None]).astype(jnp.bfloat16)
    return (kv_cache, gate_cache, read)


def solution(mesh):
    placed = (P("gr", "tp", "sp", None), P(), P(), P("gr", None, "tp", "sp"), P("gr", "sp", None))
    return jax.shard_map(
        on_device,
        mesh=mesh,
        in_specs=placed,
        out_specs=(P("gr", "sp", "tp", None), P("gr", "sp", "tp"), P("gr", "sp", None)),
        check_vma=False,
    )
```

profile of v0, /device:TPU:25, one launch (start us, length us, event | category | flops | bytes accessed | tf_op | source)
XLA Modules:
  0.0 214.8 jit_solution(17733755915182481379)
XLA Ops:
  0.6 0.0 copy-start
  0.6 5.8 %all-to-all-start.1 = ((f32[1,32,1,768]{3,2,0,1:T(1,128)}), f32[1,32,1,768]{3,2,0,1:T(1,128)S(1)}, u32[]{:S(2)}, u32[]{:S(2)}) async-start(f32[1,32,1,768]{3,2,0,1:T(1,128)} %bitcast.77), calls=%async_computation.1 | async-start | bytes 196608 | tf_op jit(solution)/shard_map/all_to_all | solution.py:62
  6.4 12.3 %copy.23 = bf16[2048,2048]{0,1:T(8,128)(2,1)} copy(bf16[2048,2048]{1,0:T(8,128)(2,1)} %param.7) | data formatting | bytes 16777216 | tf_op args[2]
  18.7 12.4 %copy.22 = bf16[2048,2048]{0,1:T(8,128)(2,1)} copy(bf16[2048,2048]{1,0:T(8,128)(2,1)} %param.6) | data formatting | bytes 16777216 | tf_op args[1]
  31.0 0.0 copy-done
  31.0 0.0 copy-start.1
  31.0 9.3 %convert_bitcast_fusion = bf16[1,32,768,64]{2,3,1,0:T(8,128)(2,1)S(1)} fusion(bf16[2048,32,64]{0,2,1:T(8,128)(2,1)} %bitcast.68, bf16[1,1,768,2048]{3,2,1,0:T(8,128)(2,1)S(1)} %copy-done), kind=kOutput, calls=%fused_computation.9 | convolution fusion | flops 6444023808 | bytes 14680064 | tf_op jit(solution)/shard_map/btd,dhe->bhte/dot_general | solution.py:45
  40.3 0.0 copy-done.1
  40.3 6.9 %convert_bitcast_fusion.1 = bf16[1,32,768,64]{2,3,1,0:T(8,128)(2,1)S(1)} fusion(bf16[2048,32,64]{0,2,1:T(8,128)(2,1)S(1)} %bitcast.67, bf16[1,1,768,2048]{3,2,1,0:T(8,128)(2,1)S(1)} %copy-done), kind=kOutput, calls=%fused_computation.10 | convolution fusion | flops 6444023808 | bytes 14680064 | tf_op jit(solution)/shard_map/btd,dhe->bhte/dot_general | solution.py:39
  47.3 3.4 %maximum_bitcast_fusion = bf16[1,32,768,128]{2,3,0,1:T(8,128)(2,1)} fusion(bf16[1,32,768,64]{2,3,1,0:T(8,128)(2,1)S(1)} %convert_bitcast_fusion, bf16[1,32,768,64]{2,3,1,0:T(8,128)(2,1)S(1)} %convert_bitcast_fusion.1), kind=kLoop, calls=%fused_computation.4 | loop fusion | flops 12582912 | bytes 12582912 | tf_op jit(solution)/shard_map/concatenate | solution.py:60
  50.6 0.0 copy-start.4
  50.6 0.0 all-to-all-done.1
  50.6 5.6 %all-to-all-start = ((bf16[1,32,768,128]{2,3,0,1:T(8,128)(2,1)}), bf16[1,32,768,128]{2,3,0,1:T(8,128)(2,1)}, u32[]{:S(2)}, u32[]{:S(2)}) async-start(bf16[1,32,768,128]{2,3,0,1:T(8,128)(2,1)} %maximum_bitcast_fusion), calls=%async_computation | async-start | bytes 12582912 | tf_op jit(solution)/shard_map/all_to_all | solution.py:61
  56.2 0.0 copy-done.4
  56.2 0.6 dynamic-slice
  57.5 0.7 reshape.234
  58.2 135.4 %all-to-all-done = bf16[1,32,768,128]{2,3,0,1:T(8,128)(2,1)} async-done(((bf16[1,32,768,128]{2,3,0,1:T(8,128)(2,1)}), bf16[1,32,768,128]{2,3,0,1:T(8,128)(2,1)}, u32[]{:S(2)}, u32[]{:S(2)}) %all-to-all-start) | async-done | bytes 6291488 | tf_op jit(solution)/shard_map/all_to_all | solution.py:61
  193.6 0.0 copy-start.3
  193.6 8.6 %copy.25 = bf16[1,4,8,768,128]{4,3,2,1,0:T(8,128)(2,1)} copy(bf16[1,4,8,768,128]{3,4,1,2,0:T(8,128)(2,1)} %bitcast.11) | data formatting | bytes 12582912 | tf_op jit(solution)/shard_map/all_to_all | solution.py:61
  202.3 0.0 copy-start.2
  202.3 0.0 copy-done.3
  202.3 4.6 %fusion.1 = f32[4,1,6144]{2,1,0:T(1,128)S(1)} fusion(bf16[1,4,6144,128]{3,2,1,0:T(8,128)(2,1)} %bitcast.69, bf16[4,64,1]{1,0,2:T(4,128)(2,1)S(1)} %bitcast.79), kind=kOutput, calls=%fused_computation.3 | convolution fusion | flops 3145728 | bytes 6390272 | tf_op jit(solution)/shard_map/bhe,bhse->bhs/dot_general | solution.py:25
  206.9 0.2 fusion.22
  207.1 0.2 fusion.12
  207.3 0.0 copy-done.2
  207.4 1.9 fusion
  209.3 0.2 dynamic-update-slice
  209.5 0.2 dynamic-update-slice.1
  209.7 2.0 all-gather.3
  211.7 2.5 %all-reduce.2 = (f32[8]{0:T(128)S(1)}, f32[8]{0:T(128)S(1)}) all-reduce(f32[8]{0:T(128)S(1)} %dynamic-update-slice, f32[8]{0:T(128)S(1)} %dynamic-update-slice.1), channel_id=3, replica_groups=mesh['gr'=2,'sp'=8,'tp'=2] {'tp'}, use_global_device_ids=true, to_apply=%add | all-reduce | flops 16 | bytes 128
  214.1 0.1 fusion.21
  214.2 0.6 fusion.18
  (4 shorter events, 0.1 us)
Async XLA Ops:
  0.6 30.4 %copy-start = (bf16[1,1,768,2048]{3,2,1,0:T(8,128)(2,1)S(1)}, bf16[1,1,768,2048]{3,2,1,0:T(8,128)(2,1)}, u32[]{:S(2)}) copy-start(bf16[1,1,768,2048]{3,2,1,0:T(8,128)(2,1)} %param.5) | copy-start | bytes 9437188
  0.6 50.0 %all-to-all-start.1 = ((f32[1,32,1,768]{3,2,0,1:T(1,128)}), f32[1,32,1,768]{3,2,0,1:T(1,128)S(1)}, u32[]{:S(2)}, u32[]{:S(2)}) async-start(f32[1,32,1,768]{3,2,0,1:T(1,128)} %bitcast.77), calls=%async_computation.1 | async-start | bytes 196608 | tf_op jit(solution)/shard_map/all_to_all | solution.py:62
  31.0 9.3 %copy-start.1 = (bf16[2048,2048]{0,1:T(8,128)(2,1)S(1)}, bf16[2048,2048]{0,1:T(8,128)(2,1)}, u32[]{:S(2)}) copy-start(bf16[2048,2048]{0,1:T(8,128)(2,1)} %copy.22) | copy-start | bytes 25165828
  50.6 5.6 %copy-start.4 = (u32[32]{0:T(128)S(1)}, u32[32]{0:T(128)}, u32[]{:S(2)}) copy-start(u32[32]{0:T(128)} %constant.21) | copy-start | bytes 388
  50.6 143.0 %all-to-all-start = ((bf16[1,32,768,128]{2,3,0,1:T(8,128)(2,1)}), bf16[1,32,768,128]{2,3,0,1:T(8,128)(2,1)}, u32[]{:S(2)}, u32[]{:S(2)}) async-start(bf16[1,32,768,128]{2,3,0,1:T(8,128)(2,1)} %maximum_bitcast_fusion), calls=%async_computation | async-start | bytes 12582912 | tf_op jit(solution)/shard_map/all_to_all | solution.py:61
  193.6 8.6 %copy-start.3 = (bf16[1,4,64]{2,1,0:T(4,128)(2,1)S(1)}, bf16[1,4,64]{2,1,0:T(4,128)(2,1)}, u32[]{:S(2)}) copy-start(bf16[1,4,64]{2,1,0:T(4,128)(2,1)} %param.9) | copy-start | bytes 1540
  202.3 5.1 %copy-start.2 = (bf16[1,4,8,768,128]{4,3,2,1,0:T(8,128)(2,1)S(1)}, bf16[1,4,8,768,128]{4,3,2,1,0:T(8,128)(2,1)}, u32[]{:S(2)}) copy-start(bf16[1,4,8,768,128]{4,3,2,1,0:T(8,128)(2,1)} %copy.25) | copy-start | bytes 18874372
where the time goes:
time: 218 us; the launch traced here: 215 us
  waiting for transfers between devices  135 us (62%)
  local copies, waits for them, and re-layouts  35 us (16%)
  matrix products  22.8 us (10%)
  starting transfers between devices  11.3 us (5%)
  other arithmetic  4.53 us (2%)
  blocking collectives  4.43 us (2%)
    all_to_all x1, waiting for transfers between devices, on_device(): lax.all_to_all(joined, 'sp', split_axis=1, concat_axis=2, tiled=True)  135 us
    unnamed x18, local copies, waits for them, and re-layouts  25.7 us
    dot_general x1, matrix products, local_project(): jnp.einsum('btd,dhe->bhte', local_rows, value_weight.reshape(width, -1, h...  9.27 us
    all_to_all x1, local copies, waits for them, and re-layouts, on_device(): lax.all_to_all(joined, 'sp', split_axis=1, concat_axis=2, tiled=True)  8.63 us
    dot_general x1, matrix products, local_project(): jnp.einsum('btd,dhe->bhte', local_rows, key_weight.reshape(width, -1, hea...  6.94 us
    all_to_all x1, starting transfers between devices, on_device(): lax.all_to_all(cum_gate, 'sp', split_axis=1, concat_axis=3, tiled=True)  5.77 us
    all_to_all x1, starting transfers between devices, on_device(): lax.all_to_all(joined, 'sp', split_axis=1, concat_axis=2, tiled=True)  5.56 us
    dot_general x1, matrix products, partial_read(): jnp.einsum('bhe,bhse->bhs', query, keys, preferred_element_type=jnp.float32)  4.64 us
  transfers between devices with their start and end apart: 2, of which 1 were waited for; matrix products, arithmetic and copies ran while one was open for 21% of the time, Pallas kernels for 0%

commit v1 on v0

v1 whole, which is shorter than its diff:
```python
import functools

import jax
import jax.numpy as jnp
from jax import lax
from jax.experimental import pallas as pl
from jax.experimental.pallas import tpu as pltpu
from jax.sharding import PartitionSpec as P

MESH = pl.DeviceIdType.MESH
LANES = 128


def partner(step, me, n):
    if n != 8:
        return lax.rem(me + 1 + step, n)
    plane, side = me // 2, lax.rem(me, 2)
    upper = plane // 2
    sign = 1 - 2 * upper
    inner = lax.rem(plane + upper, 2)
    turn = step // 2
    offset = jnp.where(turn == 0, 1, jnp.where(turn == 1, 2 - 3 * inner, 3 - inner))
    offset = jnp.where(turn == 3, 0, offset * sign)
    flip = lax.rem(step, 2)
    flip = jnp.where(turn == 3, 1 - flip, flip)
    return (plane + offset) * 2 + lax.rem(side + flip, 2)


def exchange_kernel(
    n, per_owner, tile, head,
    tokens, key_weight, value_weight, gates, query,
    kv, gate_in, result,
    rows, weights, outgoing, mine, theirs,
    row_sem, weight_sem, send_sem, recv_sem, gate_send, gate_recv, pair_sem,
):
    me = lax.axis_index("sp")
    core = lax.axis_index("tp")
    count = rows.shape[0]
    tiles = count // tile
    columns = weights.shape[3]
    group_heads = columns // head
    owners = group_heads // per_owner
    groups = n // owners

    def group_of(step):
        if owners == 1:
            return partner(step, me, n)
        return lax.rem(me // owners + 1 + step, groups)

    def load_rows(t):
        span = pl.ds(t * tile, tile)
        return pltpu.make_async_copy(tokens.at[span, :], rows.at[span, :], row_sem.at[t])

    def load_weight(step, which):
        at = pl.ds(pl.multiple_of(group_of(step) * columns, columns), columns)
        source = (key_weight, value_weight)[which]
        return pltpu.make_async_copy(
            source.at[:, at], weights.at[step, which], weight_sem.at[step, which]
        )

    load_rows(0).start()
    load_weight(0, 0).start()
    load_weight(0, 1).start()
    for t in range(1, tiles):
        load_rows(t).start()

    barrier = pltpu.get_barrier_semaphore()

    @pl.loop(1, n)
    def _(k):
        pl.semaphore_signal(
            barrier, inc=1, device_id={"sp": lax.rem(me + k, n)}, device_id_type=MESH
        )

    pl.semaphore_signal(barrier, inc=1, device_id={"tp": 1 - core}, device_id_type=MESH)
    pl.semaphore_wait(barrier, n)

    def gate_copy(owner):
        return pltpu.make_async_remote_copy(
            src_ref=gates.at[owner], dst_ref=gate_in.at[me],
            send_sem=gate_send.at[owner], recv_sem=gate_recv.at[me],
            device_id={"sp": owner}, device_id_type=MESH,
        )

    def gate_own():
        return pltpu.make_async_copy(gates.at[me], gate_in.at[me], gate_recv.at[me])

    @pl.loop(0, n - 1)
    def _(k):
        gate_copy(lax.rem(me + 1 + k, n)).start()

    gate_own().start()

    def block_copy(owner, t):
        return pltpu.make_async_remote_copy(
            src_ref=outgoing.at[owner, :, pl.ds(t * tile, tile), :],
            dst_ref=kv.at[:, pl.ds(pl.multiple_of(me * count + t * tile, tile), tile), :],
            send_sem=send_sem.at[owner, t], recv_sem=recv_sem.at[me, t],
            device_id={"sp": owner}, device_id_type=MESH,
        )

    def block_own(t):
        return pltpu.make_async_copy(
            outgoing.at[me, :, pl.ds(t * tile, tile), :],
            kv.at[:, pl.ds(pl.multiple_of(me * count + t * tile, tile), tile), :],
            recv_sem.at[me, t],
        )

    low = lax.broadcasted_iota(jnp.int32, (tile, LANES), 1) < head

    def project(step, first):
        group = group_of(step)

        if first:
            for ahead in range(1, min(3, groups)):
                load_weight(ahead, 0).start()
                load_weight(ahead, 1).start()
        else:
            @pl.when(step + 2 < groups)
            def _():
                load_weight(step + 2, 0).start()
                load_weight(step + 2, 1).start()

        load_weight(step, 0).wait()
        load_weight(step, 1).wait()
        for t in range(tiles):
            if first:
                load_rows(t).wait()
            left = rows[pl.ds(t * tile, tile), :]
            keys = jnp.dot(left, weights[step, 0], preferred_element_type=jnp.float32)
            values = jnp.dot(left, weights[step, 1], preferred_element_type=jnp.float32)
            for pair in range(columns // LANES):
                span = slice(pair * LANES, (pair + 1) * LANES)
                k, v = keys[:, span], values[:, span]
                joined = (
                    jnp.where(low, k, pltpu.roll(v, head, 1)),
                    jnp.where(low, pltpu.roll(k, head, 1), v),
                )
                for half in range(2):
                    local = pair * 2 + half
                    owner = group * owners + local // per_owner
                    outgoing[owner, local % per_owner, pl.ds(t * tile, tile), :] = joined[
                        half
                    ].astype(jnp.bfloat16)
            for j in range(owners):
                owner = group * owners + j

                @pl.when(owner != me)
                def _():
                    block_copy(owner, t).start()

                @pl.when(owner == me)
                def _():
                    block_own(t).start()

    project(0, True)

    def later(step, carry):
        project(step, False)
        return carry

    lax.fori_loop(1, groups, later, 0)

    wide = jnp.concatenate(
        [query[...].astype(jnp.float32), jnp.zeros((per_owner, LANES - head), jnp.float32)], axis=1
    ) * (head ** -0.5)
    head_row = lax.broadcasted_iota(jnp.int32, (per_owner, LANES), 0)
    tile_row = lax.broadcasted_iota(jnp.int32, (per_owner, tile), 0)
    queries = [jnp.where(head_row == h, wide, 0.0).astype(jnp.bfloat16) for h in range(per_owner)]

    @pl.loop(0, n - 1)
    def _(k):
        source = lax.rem(me + 1 + k, n)
        gate_copy(source).wait_send()
        pltpu.make_async_copy(gates.at[source], gate_in.at[source], gate_recv.at[source]).wait()

    gate_own().wait()

    def read_block(source, t, carry):
        top, total, weighted = carry
        span = pl.ds(pl.multiple_of(source * count + t * tile, tile), tile)
        pltpu.make_async_copy(
            outgoing.at[me, :, pl.ds(t * tile, tile), :], kv.at[:, span, :], recv_sem.at[source, t]
        ).wait()
        scores = None
        blocks = [kv[h, span, :] for h in range(per_owner)]
        for h in range(per_owner):
            term = lax.dot_general(
                queries[h], blocks[h], (((1,), (1,)), ((), ())), preferred_element_type=jnp.float32
            )
            scores = term if scores is None else scores + term
        gate = jnp.concatenate(
            [gate_in[source, h, :, pl.ds(t * tile, tile)] for h in range(per_owner)], axis=0
        )
        scores = scores - gate
        new_top = jnp.maximum(top, jnp.max(scores, axis=1, keepdims=True))
        scale = jnp.exp(top - new_top)
        probs = jnp.exp(scores - new_top)
        total = total * scale + jnp.sum(probs, axis=1, keepdims=True)
        weighted = weighted * scale
        for h in range(per_owner):
            picked = jnp.where(tile_row == h, probs, 0.0).astype(jnp.bfloat16)
            weighted = weighted + jnp.dot(picked, blocks[h], preferred_element_type=jnp.float32)
        return new_top, total, weighted

    carry = (
        jnp.full((per_owner, 1), -1e30, jnp.float32),
        jnp.zeros((per_owner, 1), jnp.float32),
        jnp.zeros((per_owner, LANES), jnp.float32),
    )

    for t in range(tiles):
        def from_source(k, carry, t=t):
            return read_block(partner(n - 1 - k, me, n), t, carry)

        carry = lax.fori_loop(0, n, from_source, carry)

    top, total, weighted = carry
    lane = lax.broadcasted_iota(jnp.int32, (per_owner, LANES), 1)
    packed = jnp.where(lane < head // 2, top, jnp.where(lane < head, total, weighted))
    mine[...] = packed
    swap = pltpu.make_async_remote_copy(
        src_ref=mine, dst_ref=theirs, send_sem=pair_sem.at[0], recv_sem=pair_sem.at[1],
        device_id={"tp": 1 - core}, device_id_type=MESH,
    )
    swap.start()

    @pl.loop(0, n - 1)
    def _(k):
        for t in range(tiles):
            block_copy(lax.rem(me + 1 + k, n), t).wait_send()

    swap.wait()
    other = theirs[...]
    one = jnp.where(core == 0, packed, other)
    two = jnp.where(core == 0, other, packed)
    top_one, top_two = one[:, :1], two[:, :1]
    joint = jnp.maximum(top_one, top_two)
    scale_one, scale_two = jnp.exp(top_one - joint), jnp.exp(top_two - joint)
    at = head // 2
    bottom = one[:, at:at + 1] * scale_one + two[:, at:at + 1] * scale_two
    result[...] = (one * scale_one + two * scale_two) / bottom


def finish_kernel(head, kv, gate_in, result, kv_out, gate_out, read, sem):
    heads, length = kv.shape[0], kv.shape[1]
    copies = [
        pltpu.make_async_copy(kv.at[h], kv_out.at[h], sem.at[h]) for h in range(heads)
    ]
    for copy in copies:
        copy.start()
    n, count = gate_in.shape[0], gate_in.shape[3]
    for source in range(n):
        gate_out[:, source * count:(source + 1) * count] = jnp.concatenate(
            [gate_in[source, h] for h in range(heads)], axis=0
        )
    read[...] = pltpu.roll(result[...], head, 1)[:, :head].astype(jnp.bfloat16)
    for copy in copies:
        copy.wait()


def on_device(n, tokens, key_weight, value_weight, cum_gate, query):
    _, _, count, width = tokens.shape
    heads = cum_gate.shape[1]
    per_owner, head = query.shape[1], query.shape[2]
    tile = 256 if count % 256 == 0 else count
    columns = max(per_owner * head, LANES)
    groups = heads * head // columns
    tiles = count // tile
    any_space = pl.BlockSpec(memory_space=pl.ANY)
    vmem = pl.BlockSpec(memory_space=pltpu.VMEM)
    kv, gate_in, result = pl.pallas_call(
        functools.partial(exchange_kernel, n, per_owner, tile, head),
        name="exchange",
        out_shape=(
            pltpu.VMEM((per_owner, n * count, 2 * head), jnp.bfloat16),
            pltpu.VMEM((n, per_owner, 1, count), jnp.float32),
            pltpu.VMEM((per_owner, 2 * head), jnp.float32),
        ),
        in_specs=[any_space] * 4 + [vmem],
        out_specs=(vmem, vmem, vmem),
        scratch_shapes=[
            pltpu.VMEM((count, width), jnp.bfloat16),
            pltpu.VMEM((groups, 2, width, columns), jnp.bfloat16),
            pltpu.VMEM((n, per_owner, count, 2 * head), jnp.bfloat16),
            pltpu.VMEM((per_owner, 2 * head), jnp.float32),
            pltpu.VMEM((per_owner, 2 * head), jnp.float32),
            pltpu.SemaphoreType.DMA((tiles,)),
            pltpu.SemaphoreType.DMA((groups, 2)),
            pltpu.SemaphoreType.DMA((n, tiles)),
            pltpu.SemaphoreType.DMA((n, tiles)),
            pltpu.SemaphoreType.DMA((n,)),
            pltpu.SemaphoreType.DMA((n,)),
            pltpu.SemaphoreType.DMA((2,)),
        ],
        compiler_params=pltpu.CompilerParams(
            collective_id=0, has_side_effects=True, vmem_limit_bytes=56 * 1024 * 1024
        ),
    )(
        tokens.reshape(count, width),
        key_weight,
        value_weight,
        cum_gate.reshape(n, per_owner, 1, count),
        query.reshape(per_owner, head),
    )
    kv_out, gate_out, read = pl.pallas_call(
        functools.partial(finish_kernel, head),
        name="finish",
        out_shape=(
            jax.ShapeDtypeStruct((per_owner, n * count, 2 * head), jnp.bfloat16),
            jax.ShapeDtypeStruct((per_owner, n * count), jnp.float32),
            jax.ShapeDtypeStruct((per_owner, head), jnp.bfloat16),
        ),
        in_specs=[vmem, vmem, vmem],
        out_specs=(any_space, vmem, vmem),
        scratch_shapes=[pltpu.SemaphoreType.DMA((per_owner,))],
        compiler_params=pltpu.CompilerParams(vmem_limit_bytes=16 * 1024 * 1024),
    )(kv, gate_in, result)
    return kv_out[None], gate_out[None], read[None]


def solution(mesh):
    placed = (P("gr", "tp", "sp", None), P(), P(), P("gr", None, "tp", "sp"), P("gr", "sp", None))
    return jax.shard_map(
        functools.partial(on_device, mesh.shape["sp"]),
        mesh=mesh,
        in_specs=placed,
        out_specs=(P("gr", "sp", "tp", None), P("gr", "sp", "tp"), P("gr", "sp", None)),
        check_vma=False,
    )
```

time: 218 us -> 167 us (0.77)
  Pallas kernels: 0 us -> 164 us
  waiting for transfers between devices: 135 us -> 0 us
  local copies, waits for them, and re-layouts: 35 us -> 0 us
  matrix products: 22.8 us -> 0 us
  starting transfers between devices: 11.3 us -> 0 us
  other arithmetic: 4.53 us -> 0 us
  blocking collectives: 4.43 us -> 0 us
    pallas_call x0 -> x2, Pallas kernels: none -> 164 us  [the longest x1 161 us: on_device(): pl.pallas_call(functools.partial(exchange_kernel, n, per_owner, tile, hea...]
    all_to_all x2 -> x0, waiting for transfers between devices: 135 us -> none  [the longest x1 135 us: on_device(): lax.all_to_all(joined, 'sp', split_axis=1, concat_axis=2, tiled=True)]
    unnamed x18 -> x0, local copies, waits for them, and re-layouts: 25.7 us -> none
    dot_general x4 -> x0, matrix products: 22.8 us -> none  [the longest x1 9.27 us: local_project(): jnp.einsum('btd,dhe->bhte', local_rows, value_weight.reshape(width, -1, h...]
    all_to_all x2 -> x0, starting transfers between devices: 11.3 us -> none  [the longest x1 5.77 us: on_device(): lax.all_to_all(cum_gate, 'sp', split_axis=1, concat_axis=3, tiled=True)]
    all_to_all x2 -> x0, local copies, waits for them, and re-layouts: 8.65 us -> none  [the longest x1 8.63 us: on_device(): lax.all_to_all(joined, 'sp', split_axis=1, concat_axis=2, tiled=True)]
    concatenate x1 -> x0, other arithmetic: 3.36 us -> none  [on_device(): joined = jnp.concatenate([key_part, value_part], axis=-1)]
    unnamed x1 -> x0, blocking collectives: 2.45 us -> none
  transfers between devices with their start and end apart: 2 -> 0, of which waited for: 1 -> 0; matrix products, arithmetic and copies ran while one was open for 21% -> 0% of each run, Pallas kernels for 0% -> 0%
where the time goes in v1:
time: 167 us; the launch traced here: 165 us
  Pallas kernels  164 us (98%)
    pallas_call x1, Pallas kernels, on_device(): pl.pallas_call(functools.partial(exchange_kernel, n, per_owner, tile, hea...  161 us
    pallas_call x1, Pallas kernels, on_device(): pl.pallas_call(functools.partial(finish_kernel, head), name='finish', out...  3.41 us

profile of v1, /device:TPU:25, one launch (start us, length us, event | category | flops | bytes accessed | tf_op | source)
XLA Modules:
  0.0 164.7 jit_solution(14503322600027565067)
XLA Ops:
  0.6 160.7 %exchange.1 = (bf16[4,6144,128]{2,1,0:T(8,128)(2,1)S(1)}, f32[8,4,1,768]{3,2,1,0:T(1,128)S(1)}, f32[4,128]{1,0:T(4,128)S(1)}) custom-call(bf16[768,2048]{1,0:T(8,128)(2,1)} %bitcast.6, bf16[2048,2048]{1,0:T(8,128)(2,1)} %key_weight.1, bf16[2048,2048]{1,0:T(8,128)(2,1)} %value_weight.1, f32[8,4,1,768]{3,2,1,0:T(1,128)} %bitcast.7, bf16[4,64]{1,0:T(4,128)(2,1)} %bitcast.8), custom_call_target="tpu_custom_call" | custom-call | tf_op jit(solution)/shard_map/exchange/pallas_call | solution.py:272
  161.3 3.4 %finish.1 = (bf16[4,6144,128]{2,1,0:T(8,128)(2,1)}, f32[4,6144]{1,0:T(4,128)}, bf16[4,64]{1,0:T(4,128)(2,1)}) custom-call(bf16[4,6144,128]{2,1,0:T(8,128)(2,1)S(1)} %get-tuple-element.9.kv, f32[8,4,1,768]{3,2,1,0:T(1,128)S(1)} %get-tuple-element.10.gate_in, f32[4,128]{1,0:T(4,128)S(1)} %get-tuple-element.11.result), custom_call_target="tpu_custom_call" | custom-call | tf_op jit(solution)/shard_map/finish/pallas_call | solution.py:306

commit v2 on v1

--- a/solution.py
+++ b/solution.py
@@ -12,18 +12,11 @@
 
 
 def partner(step, me, n):
-    if n != 8:
+    if n % 2:
         return lax.rem(me + 1 + step, n)
-    plane, side = me // 2, lax.rem(me, 2)
-    upper = plane // 2
-    sign = 1 - 2 * upper
-    inner = lax.rem(plane + upper, 2)
-    turn = step // 2
-    offset = jnp.where(turn == 0, 1, jnp.where(turn == 1, 2 - 3 * inner, 3 - inner))
-    offset = jnp.where(turn == 3, 0, offset * sign)
-    flip = lax.rem(step, 2)
-    flip = jnp.where(turn == 3, 1 - flip, flip)
-    return (plane + offset) * 2 + lax.rem(side + flip, 2)
+    turn, flip = step // 2, lax.rem(step, 2)
+    flip = jnp.where(turn == n // 2 - 1, 1 - flip, flip)
+    return lax.rem(me // 2 + 1 + turn, n // 2) * 2 + lax.rem(me + flip, 2)
 
 
 def exchange_kernel(

time: 167 us -> 151 us (0.904); the launches traced: 165 us -> 151 us
  Pallas kernels: 164 us -> 150 us
    pallas_call x1, Pallas kernels: 161 us -> 147 us  [on_device(): pl.pallas_call(functools.partial(exchange_kernel, n, per_owner, tile, hea...]
where the time goes in v2:
time: 151 us
  Pallas kernels  150 us (99%)
    pallas_call x1, Pallas kernels, on_device(): pl.pallas_call(functools.partial(exchange_kernel, n, per_owner, tile, hea...  147 us
    pallas_call x1, Pallas kernels, on_device(): pl.pallas_call(functools.partial(finish_kernel, head), name='finish', out...  3.41 us

profile of v2, /device:TPU:25, one launch (start us, length us, event | category | flops | bytes accessed | tf_op | source)
XLA Modules:
  0.0 150.6 jit_solution(14540696441196388960)
XLA Ops:
  0.6 146.6 %exchange.1 = (bf16[4,6144,128]{2,1,0:T(8,128)(2,1)S(1)}, f32[8,4,1,768]{3,2,1,0:T(1,128)S(1)}, f32[4,128]{1,0:T(4,128)S(1)}) custom-call(bf16[768,2048]{1,0:T(8,128)(2,1)} %bitcast.6, bf16[2048,2048]{1,0:T(8,128)(2,1)} %key_weight.1, bf16[2048,2048]{1,0:T(8,128)(2,1)} %value_weight.1, f32[8,4,1,768]{3,2,1,0:T(1,128)} %bitcast.7, bf16[4,64]{1,0:T(4,128)(2,1)} %bitcast.8), custom_call_target="tpu_custom_call" | custom-call | tf_op jit(solution)/shard_map/exchange/pallas_call | solution.py:265
  147.2 3.4 %finish.1 = (bf16[4,6144,128]{2,1,0:T(8,128)(2,1)}, f32[4,6144]{1,0:T(4,128)}, bf16[4,64]{1,0:T(4,128)(2,1)}) custom-call(bf16[4,6144,128]{2,1,0:T(8,128)(2,1)S(1)} %get-tuple-element.9.kv, f32[8,4,1,768]{3,2,1,0:T(1,128)S(1)} %get-tuple-element.10.gate_in, f32[4,128]{1,0:T(4,128)S(1)} %get-tuple-element.11.result), custom_call_target="tpu_custom_call" | custom-call | tf_op jit(solution)/shard_map/finish/pallas_call | solution.py:299
